TPU v7x, 32 devices: a whole 2x2x4 slice. The times are simulated.
32 devices in a mesh: ep: 16 (over z, y, x), tp: 2 (over core).
Axes of the slice: x: 2, y: 2, z: 4, core: 2. Of those that a mesh axis runs over, the one named last changes fastest.
Arguments:
- tokens: bfloat16 [256, 2048], P('ep', 'tp'), may hold values from -6 to 6
- state: float32 [256, 4, 128, 128], P('ep', 'tp'), may hold values from -4 to 4
- norm_mix: float32 [2048], replicated, may hold values from 0.1 to 1.9
- w_query: bfloat16 [2048, 512], P(None, 'tp'), may hold values from -0.125 to 0.125
- w_key: bfloat16 [2048, 512], P(None, 'tp'), may hold values from -0.125 to 0.125
- w_value: bfloat16 [2048, 512], P(None, 'tp'), may hold values from -0.125 to 0.125
- w_out: bfloat16 [512, 2048], P('tp'), may hold values from -0.25 to 0.25
- norm_ffn: float32 [2048], P('tp'), may hold values from 0.1 to 1.9
- gate_vector: bfloat16 [2048], P('tp'), may hold values from -0.125 to 0.125
- dense_gate: bfloat16 [2048, 2816], P('tp', 'ep'), may hold values from -0.125 to 0.125
- dense_up: bfloat16 [2048, 2816], P('tp', 'ep'), may hold values from -0.125 to 0.125
- dense_down: bfloat16 [2816, 2048], P('ep', 'tp'), may hold values from -0.109375 to 0.109375
- exp_gate: bfloat16 [16, 2048, 1408], P('ep', None, 'tp'), may hold values from -0.125 to 0.125
- exp_up: bfloat16 [16, 2048, 1408], P('ep', None, 'tp'), may hold values from -0.125 to 0.125
- exp_down: bfloat16 [16, 1408, 2048], P('ep', 'tp'), may hold values from -0.109375 to 0.109375
- routes: int32 [256, 2], P('ep'), may hold values from 0 to 7, all different within a row; in each aligned block of 16 rows (0 to 15, 16 to 31, ...) at most 5 rows name the same one
- route_w: bfloat16 [256, 2], P('ep'), may hold values from 0.099609375 to 1
Outputs:
- mixed: bfloat16 [256, 2048], P('ep', 'tp')
- new_state: float32 [256, 4, 128, 128], P('ep', 'tp')
Inputs may be any that keep to these rules, and one draw needn't show every extreme that they name: `routes`: each row names 2 different experts. Within the rows of one device (aligned blocks of 16 rows) no expert is named by more than 5 rows, a bound that some blocks reach.
All inputs are finite; a program needn't handle non-finite values.
Results may differ from a plain program's by a relative error of at most 0.014.
Values may be sent and summed in bfloat16 or wider, within the bound.
A program may use at most 128 MiB of HBM per device.

v0:
```python
import jax
import jax.numpy as jnp
from jax import lax
from jax.sharding import PartitionSpec as P

EXPERTS = 8
CAP = 5
epsilon = 1e-06


def route_tables(routes, route_w):
    onehot = (routes[:, :, None] == jnp.arange(EXPERTS, dtype=jnp.int32)[None, None, :]).astype(
        jnp.float32
    )
    member = jnp.sum(onehot, axis=1)
    weight = jnp.sum(onehot * route_w.astype(jnp.float32)[:, :, None], axis=1)
    place = jnp.cumsum(member, axis=0) - member
    slot_ids = jnp.arange(CAP, dtype=jnp.float32)
    select = member.T[:, None, :] * (place.T[:, None, :] == slot_ids[None, :, None]).astype(
        jnp.float32
    )
    return (select, weight)


def expert_math(flat_rows, weights):
    gate_pre = jnp.dot(flat_rows, weights[0], preferred_element_type=jnp.float32)
    up_part = jnp.dot(flat_rows, weights[1], preferred_element_type=jnp.float32)
    hidden = (jax.nn.silu(gate_pre) * up_part).astype(jnp.bfloat16)
    return jnp.dot(hidden, weights[2], preferred_element_type=jnp.float32)


def expert_apply(slot_rows, weights):
    full_rows = lax.all_gather(slot_rows, "tp", axis=2, tiled=True)
    row_count = full_rows.shape[0] * full_rows.shape[1]
    partial_value = expert_math(full_rows.reshape(row_count, full_rows.shape[2]), weights)
    summed = lax.psum_scatter(
        partial_value.astype(jnp.bfloat16), "tp", scatter_dimension=1, tiled=True
    ).astype(jnp.float32)
    return summed.reshape(slot_rows.shape[0], slot_rows.shape[1], summed.shape[1])


def body(
    tokens,
    state,
    norm_mix,
    w_query,
    w_key,
    w_value,
    w_out,
    norm_ffn,
    gate_vector,
    dense_gate,
    dense_up,
    dense_down,
    exp_gate,
    exp_up,
    exp_down,
    routes,
    route_w,
):
    highest = lax.Precision.HIGHEST
    row_count, half_width = tokens.shape
    heads_here, head_size = (state.shape[1], state.shape[2])
    weights = (exp_gate[0], exp_up[0], exp_down[0])
    full_x = lax.all_gather(tokens, "tp", axis=1, tiled=True)
    width = full_x.shape[1]
    full_f = full_x.astype(jnp.float32)
    normed = (
        full_f
        * lax.rsqrt(jnp.sum(full_f * full_f, axis=1, keepdims=True) / width + epsilon)
        * norm_mix
    ).astype(jnp.bfloat16)
    query = jnp.dot(normed, w_query, preferred_element_type=jnp.float32).astype(jnp.bfloat16)
    key_rows = jnp.dot(normed, w_key, preferred_element_type=jnp.float32).astype(jnp.bfloat16)
    value_rows = jnp.dot(normed, w_value, preferred_element_type=jnp.float32).astype(jnp.bfloat16)
    query3 = query.astype(jnp.float32).reshape(row_count, heads_here, head_size)
    key3 = key_rows.astype(jnp.float32).reshape(row_count, heads_here, head_size) * head_size ** (
        -0.5
    )
    value3 = value_rows.astype(jnp.float32).reshape(row_count, heads_here, head_size)
    head_ids = (lax.axis_index("tp") * heads_here + jnp.arange(heads_here, dtype=jnp.int32)).astype(
        jnp.float32
    )
    decay = 1.0 - jnp.exp2(-3.0 - 2.0 * head_ids)
    new_state = decay[None, :, None, None] * state + jnp.einsum(
        "shd,she->shde", key3, value3, precision=highest
    )
    read = jnp.einsum("shd,shde->she", query3, new_state, precision=highest)
    centre = jnp.mean(read, axis=2, keepdims=True)
    spread = jnp.mean(jnp.square(read - centre), axis=2, keepdims=True)
    heads_out = (
        ((read - centre) * lax.rsqrt(spread + epsilon))
        .astype(jnp.bfloat16)
        .reshape(row_count, heads_here * head_size)
    )
    mix_part = jnp.dot(heads_out, w_out, preferred_element_type=jnp.float32)
    mix_half = lax.psum_scatter(
        mix_part.astype(jnp.bfloat16), "tp", scatter_dimension=1, tiled=True
    ).astype(jnp.float32)
    after = (tokens.astype(jnp.float32) + mix_half).astype(jnp.bfloat16)
    after_hf = after.astype(jnp.float32)
    squares = lax.psum(jnp.sum(after_hf * after_hf, axis=1, keepdims=True), "tp")
    after_f = after.astype(jnp.float32)
    normed2 = (after_f * lax.rsqrt(squares / width + epsilon) * norm_ffn).astype(jnp.bfloat16)
    all_rows = lax.all_gather(normed2, "ep", axis=0, tiled=True)
    dense_pre = jnp.dot(all_rows, dense_gate, preferred_element_type=jnp.float32)
    up_pre = jnp.dot(all_rows, dense_up, preferred_element_type=jnp.float32)
    logit = jnp.dot(all_rows, gate_vector, preferred_element_type=jnp.float32)
    dense_pre, up_pre, logit = (
        lax.psum(dense_pre.astype(jnp.bfloat16), "tp").astype(jnp.float32),
        lax.psum(up_pre.astype(jnp.bfloat16), "tp").astype(jnp.float32),
        lax.psum(logit.astype(jnp.bfloat16), "tp").astype(jnp.float32),
    )
    dense_hidden = (jax.nn.sigmoid(logit)[:, None] * jax.nn.silu(dense_pre) * up_pre).astype(
        jnp.bfloat16
    )
    ep_count = lax.axis_size("ep")
    group_size = ep_count // EXPERTS
    select, weight = route_tables(routes, route_w)
    outgoing = jnp.einsum(
        "ecr,rd->ecd", select.astype(jnp.bfloat16), normed2, preferred_element_type=jnp.float32
    ).astype(jnp.bfloat16)
    outgoing = jnp.repeat(outgoing, group_size, axis=0)
    served = expert_apply(
        lax.all_to_all(outgoing, "ep", split_axis=0, concat_axis=0, tiled=True), weights
    )
    returned = lax.all_to_all(
        served.astype(jnp.bfloat16), "ep", split_axis=0, concat_axis=0, tiled=True
    ).astype(served.dtype)
    per_expert = jnp.sum(returned.reshape(EXPERTS, group_size, CAP, half_width), axis=1)
    local_moe = jnp.einsum(
        "ecr,ecd->rd", select * weight.T[:, None, :], per_expert, precision=highest
    )
    value = jnp.dot(dense_hidden, dense_down, preferred_element_type=jnp.float32)
    combined = lax.psum_scatter(value, "ep", scatter_dimension=0, tiled=True)
    return ((after_f + local_moe + combined).astype(jnp.bfloat16), new_state)


def solution(mesh):
    return jax.shard_map(
        body,
        mesh=mesh,
        in_specs=(
            P("ep", "tp"),
            P("ep", "tp", None, None),
            P(),
            P(None, "tp"),
            P(None, "tp"),
            P(None, "tp"),
            P("tp", None),
            P("tp"),
            P("tp"),
            P("tp", "ep"),
            P("tp", "ep"),
            P("ep", "tp"),
            P("ep", None, "tp"),
            P("ep", None, "tp"),
            P("ep", "tp", None),
            P("ep", None),
            P("ep", None),
        ),
        out_specs=(P("ep", "tp"), P("ep", "tp", None, None)),
        check_vma=False,
    )
```

profile of v0, /device:TPU:0, one launch (start us, length us, event | category | flops | bytes accessed | tf_op | source)
XLA Modules:
  0.0 210.0 jit_solution(15320848404340629431)
XLA Ops:
  7.2 2.3 %all_gather.9 = bf16[16,2048]{1,0:T(8,128)(2,1)S(1)} all-gather(bf16[16,1024]{1,0:T(8,128)(2,1)} %param.17), channel_id=1, replica_groups=mesh['ep'=16,'tp'=2] {'tp'}, dimensions={1}, use_global_device_ids=true | all-gather | bytes 98304 | tf_op jit(solution)/shard_map/all_gather | solution.py:65
  9.7 1.5 convolution_convert_fusion.6
  11.3 1.5 fusion.18
  12.8 1.5 fusion.20
  14.4 2.0 multiply_add_fusion
  16.4 1.3 copy-done.1
  19.2 2.1 convolution_convert_fusion
  21.6 10.0 %reduce-scatter.4.cloned.1.call-done = bf16[16,1024]{1,0:T(8,128)(2,1)} async-done(((bf16[16,2048]{1,0:T(8,128)(2,1)}), bf16[16,1024]{1,0:T(8,128)(2,1)}) %reduce-scatter.4.cloned.1.call-update) | async-done | bytes 32784 | tf_op jit(solution)/shard_map/reduce_scatter | solution.py:97
  32.5 2.5 %psum.28 = f32[16,1]{0,1:T(1,128)S(1)} all-reduce(f32[16,1]{0,1:T(1,128)S(1)} %bitcast.72), channel_id=1, replica_groups=mesh['ep'=16,'tp'=2] {'tp'}, use_global_device_ids=true, to_apply=%region_8.0 | all-reduce | flops 16 | bytes 128 | tf_op jit(solution)/shard_map/psum | solution.py:102
  35.8 44.0 %all_gather.11 = bf16[256,1024]{1,0:T(8,128)(2,1)S(1)} all-gather(bf16[16,1024]{1,0:T(8,128)(2,1)S(1)} %fusion.45), channel_id=1, replica_groups=mesh['ep'=16,'tp'=2] {'ep'}, dimensions={0}, use_global_device_ids=true | all-gather | bytes 557056 | tf_op jit(solution)/shard_map/all_gather | solution.py:105
  80.7 4.2 %all-to-all-start = ((bf16[16,5,1024]{2,1,0:T(8,128)(2,1)}), bf16[16,5,1024]{2,1,0:T(8,128)(2,1)}, u32[]{:S(2)}, u32[]{:S(2)}) async-start(bf16[16,5,1024]{2,1,0:T(8,128)(2,1)} %bitcast.63), calls=%async_computation.1 | async-start | bytes 524288 | tf_op jit(solution)/shard_map/all_to_all | solution.py:125
  84.9 1.9 convolution_convert_fusion.1
  86.9 2.0 convolution_convert_fusion.2
  88.9 4.5 %all-to-all-done = bf16[16,5,1024]{2,1,0:T(8,128)(2,1)} async-done(((bf16[16,5,1024]{2,1,0:T(8,128)(2,1)}), bf16[16,5,1024]{2,1,0:T(8,128)(2,1)}, u32[]{:S(2)}, u32[]{:S(2)}) %all-to-all-start) | async-done | bytes 163872 | tf_op jit(solution)/shard_map/all_to_all | solution.py:125
  93.4 3.8 %all_gather.10 = bf16[16,5,2048]{2,1,0:T(8,128)(2,1)} all-gather(bf16[16,5,1024]{2,1,0:T(8,128)(2,1)} %all-to-all-done), channel_id=1, replica_groups=mesh['ep'=16,'tp'=2] {'tp'}, dimensions={2}, use_global_device_ids=true | all-gather | bytes 491520 | tf_op jit(solution)/shard_map/all_gather | solution.py:33
  97.2 1.9 reshape.74
  99.1 3.6 %fusion.4 = f32[80,704]{1,0:T(8,128)} fusion(bf16[80,2048]{1,0:T(8,128)(2,1)} %reshape.74, bf16[1,2048,704]{1,2,0:T(8,128)(2,1)} %param.29), kind=kOutput, calls=%fused_computation.4 | convolution fusion | flops 230686720 | bytes 3436544 | tf_op jit(solution)/shard_map/dot_general | solution.py:26
  102.7 4.5 %fusion.6 = bf16[80,2048]{1,0:T(8,128)(2,1)} fusion(bf16[1,704,2048]{2,1,0:T(8,128)(2,1)S(1)} %copy-done, bf16[80,2048]{1,0:T(8,128)(2,1)} %reshape.74, bf16[1,2048,704]{1,2,0:T(8,128)(2,1)} %param.30, f32[80,704]{1,0:T(8,128)} %fusion.4), kind=kOutput, calls=%fused_computation.6 | convolution fusion | flops 461875200 | bytes 6647808 | tf_op jit(solution)/shard_map/dot_general | solution.py:29
  107.6 2.5 %psum.29 = bf16[256]{0:T(256)(128)(2,1)S(1)} all-reduce(bf16[256]{0:T(256)(128)(2,1)S(1)} %convert_element_type.119), channel_id=1, replica_groups=mesh['ep'=16,'tp'=2] {'tp'}, use_global_device_ids=true, to_apply=%region_11.12 | all-reduce | flops 256 | bytes 1024 | tf_op jit(solution)/shard_map/psum | solution.py:112
  110.1 2.4 %fusion.39 = f32[256,1024]{1,0:T(8,128)} fusion(bf16[176,1024]{1,0:T(8,128)(2,1)} %param.28, bf16[256,176]{0,1:T(8,128)(2,1)} %get-tuple-element.4, bf16[256,176]{0,1:T(8,128)(2,1)} %get-tuple-element.5, f32[256]{0:T(256)S(1)} %add_divide_fusion), kind=kOutput, calls=%fused_computation.47 | convolution fusion | flops 92680192 | bytes 1590272 | tf_op jit(solution)/shard_map/dot_general | solution.py:134
  112.5 7.0 %reduce-scatter.6.cloned.1.call-done = bf16[80,1024]{1,0:T(8,128)(2,1)} async-done(((bf16[80,2048]{1,0:T(8,128)(2,1)}), bf16[80,1024]{1,0:T(8,128)(2,1)}) %reduce-scatter.6.cloned.1.call-update) | async-done | bytes 163856 | tf_op jit(solution)/shard_map/reduce_scatter | solution.py:36
  120.6 18.1 %all_to_all.10 = bf16[16,5,1024]{2,1,0:T(8,128)(2,1)S(1)} all-to-all(bf16[16,5,1024]{2,1,0:T(8,128)(2,1)S(1)} %convert_element_type.118), channel_id=1, replica_groups=mesh['ep'=16,'tp'=2] {'ep'}, dimensions={0} | all-to-all | bytes 327680 | tf_op jit(solution)/shard_map/all_to_all | solution.py:127
  138.8 63.0 %reduce-scatter.8.cloned.1.call-done = f32[16,1024]{1,0:T(8,128)} async-done(((f32[256,1024]{1,0:T(8,128)}), f32[16,1024]{1,0:T(8,128)}) %reduce-scatter.8.cloned.1.call-update) | async-done | bytes 65552 | tf_op jit(solution)/shard_map/reduce_scatter | solution.py:135
  201.7 1.8 fusion.17
  (54 shorter events, 6.0 us)
Async XLA Ops:
  7.2 95.6 %copy-start = (bf16[1,704,2048]{2,1,0:T(8,128)(2,1)S(1)}, bf16[1,704,2048]{2,1,0:T(8,128)(2,1)}, u32[]{:S(2)}) copy-start(bf16[1,704,2048]{2,1,0:T(8,128)(2,1)} %param.31) | copy-start | bytes 8650756
  7.2 24.4 %reduce-scatter.4.cloned.1.call-start = ((), (), s32[]{:S(2)}) async-start(), calls=%async_computation.5 | async-start | bytes 98304 | tf_op jit(solution)/shard_map/reduce_scatter | solution.py:97
  14.4 6.9 %copy-start.5 = (bf16[1024]{0:T(1024)(128)(2,1)S(1)}, bf16[1024]{0:T(1024)(128)(2,1)}, u32[]{:S(2)}) copy-start(bf16[1024]{0:T(1024)(128)(2,1)} %param.25) | copy-start | bytes 6148
  14.4 7.0 %copy-start.7 = (bf16[16,2]{0,1:T(2,128)(2,1)S(1)}, bf16[16,2]{0,1:T(2,128)(2,1)}, u32[]{:S(2)}) copy-start(bf16[16,2]{0,1:T(2,128)(2,1)} %param.33) | copy-start | bytes 196
  14.4 7.0 %copy-start.6 = (s32[16,2]{0,1:T(2,128)S(1)}, s32[16,2]{0,1:T(2,128)}, u32[]{:S(2)}) copy-start(s32[16,2]{0,1:T(2,128)} %param.32) | copy-start | bytes 388
  14.4 17.2 %copy-start.2 = (bf16[16,1024]{1,0:T(8,128)(2,1)S(1)}, bf16[16,1024]{1,0:T(8,128)(2,1)}, u32[]{:S(2)}) copy-start(bf16[16,1024]{1,0:T(8,128)(2,1)} %param.17) | copy-start | bytes 98308
  14.4 20.5 %copy-start.4 = (f32[1024]{0:T(1024)S(1)}, f32[1024]{0:T(1024)}, u32[]{:S(2)}) copy-start(f32[1024]{0:T(1024)} %param.24) | copy-start | bytes 12292
  16.4 1.3 copy-start.1
  80.7 12.7 %all-to-all-start = ((bf16[16,5,1024]{2,1,0:T(8,128)(2,1)}), bf16[16,5,1024]{2,1,0:T(8,128)(2,1)}, u32[]{:S(2)}, u32[]{:S(2)}) async-start(bf16[16,5,1024]{2,1,0:T(8,128)(2,1)} %bitcast.63), calls=%async_computation.1 | async-start | bytes 524288 | tf_op jit(solution)/shard_map/all_to_all | solution.py:125
  84.9 25.2 %all-reduce.3.cloned.1.call-start = ((), (), s32[]{:S(2)}) async-start(), calls=%async_computation.8 | async-start | bytes 360448 | tf_op jit(solution)/shard_map/psum | solution.py:111
  88.9 30.7 %reduce-scatter.6.cloned.1.call-start = ((), (), s32[]{:S(2)}) async-start(), calls=%async_computation.6 | async-start | bytes 491520 | tf_op jit(solution)/shard_map/reduce_scatter | solution.py:36
  107.2 94.5 %copy-start.3 = (bf16[16,1024]{1,0:T(8,128)(2,1)S(1)}, bf16[16,1024]{1,0:T(8,128)(2,1)}, u32[]{:S(2)}) copy-start(bf16[16,1024]{1,0:T(8,128)(2,1)} %reduce-scatter.4.cloned.1.call-done) | copy-start | bytes 98308
  107.3 94.4 %reduce-scatter.8.cloned.1.call-start = ((), (), s32[]{:S(2)}) async-start(), calls=%async_computation.7 | async-start | bytes 1114112 | tf_op jit(solution)/shard_map/reduce_scatter | solution.py:135
Sparse Core Ops, SparseCore 0:
  21.4 10.1 reduce-scatter.3
  89.0 19.2 all-reduce.2
  110.6 8.9 reduce-scatter.5
  121.7 79.9 reduce-scatter.7
where the time goes:
time: 211 us; the launch traced here: 210 us
  waiting for transfers between devices  84.5 us (40%)
  blocking collectives  73.3 us (35%)
  matrix products  24.3 us (12%)
  between operations  14 us (7%)
  local copies, waits for them, and re-layouts  5.22 us (2%)
  starting transfers between devices  4.35 us (2%)
  other arithmetic  4.33 us (2%)
    reduce_scatter x1, waiting for transfers between devices, body(): combined = lax.psum_scatter(value, 'ep', scatter_dimension=0, tiled=True)  63 us
    all_gather x1, blocking collectives, body(): all_rows = lax.all_gather(normed2, 'ep', axis=0, tiled=True)  44 us
    all_to_all x1, blocking collectives, body(): lax.all_to_all(served.astype(jnp.bfloat16), 'ep', split_axis=0, concat_ax...  18.1 us
    reduce_scatter x1, waiting for transfers between devices, body(): lax.psum_scatter(mix_part.astype(jnp.bfloat16), 'tp', scatter_dimension=1...  10 us
    reduce_scatter x1, waiting for transfers between devices, expert_apply(): lax.psum_scatter(partial_value.astype(jnp.bfloat16), 'tp', scatter_dimens...  7.02 us
    dot_general x1, matrix products, expert_math(): return jnp.dot(hidden, weights[2], preferred_element_type=jnp.float32)  4.51 us
    all_to_all x1, waiting for transfers between devices, body(): lax.all_to_all(outgoing, 'ep', split_axis=0, concat_axis=0, tiled=True)  4.47 us
  transfers between devices with their start and end apart: 5, of which 4 were waited for; matrix products, arithmetic and copies ran while one was open for 8% of the time, Pallas kernels for 0%

commit v1 on v0

--- a/solution.py
+++ b/solution.py
@@ -102,7 +102,12 @@
     squares = lax.psum(jnp.sum(after_hf * after_hf, axis=1, keepdims=True), "tp")
     after_f = after.astype(jnp.float32)
     normed2 = (after_f * lax.rsqrt(squares / width + epsilon) * norm_ffn).astype(jnp.bfloat16)
-    all_rows = lax.all_gather(normed2, "ep", axis=0, tiled=True)
+    ring = [normed2]
+    for hop in range(15):
+        ring.append(lax.ppermute(ring[-1], "ep", [(dev, (dev + 1) % 16) for dev in range(16)]))
+    all_rows = jnp.roll(
+        jnp.concatenate(ring[::-1], axis=0), (lax.axis_index("ep") + 1) * ring[0].shape[0], axis=0
+    )
     dense_pre = jnp.dot(all_rows, dense_gate, preferred_element_type=jnp.float32)
     up_pre = jnp.dot(all_rows, dense_up, preferred_element_type=jnp.float32)
     logit = jnp.dot(all_rows, gate_vector, preferred_element_type=jnp.float32)

time: 211 us -> 278 us (1.32)
  waiting for transfers between devices: 84.5 us -> 185 us
  blocking collectives: 73.3 us -> 27.7 us
  starting transfers between devices: 4.35 us -> 11 us
  local copies, waits for them, and re-layouts: 5.22 us -> 10.6 us
    ppermute x0 -> x15, waiting for transfers between devices: none -> 96.7 us  [body(): lax.ppermute(ring[-1], 'ep', [(dev, (dev + 1) % 16) for dev in range(16)])]
    all_gather x1 -> x0, blocking collectives: 44 us -> none  [body(): all_rows = lax.all_gather(normed2, 'ep', axis=0, tiled=True)]
    psum x1, waiting for transfers between devices: 0.01 us -> 6.51 us  [body(): lax.psum(up_pre.astype(jnp.bfloat16), 'tp').astype(jnp.float32)]
    unnamed x17 -> x106, local copies, waits for them, and re-layouts: 1.36 us -> 7.5 us
    all_to_all x1, waiting for transfers between devices: 4.47 us -> 0.01 us  [body(): lax.all_to_all(outgoing, 'ep', split_axis=0, concat_axis=0, tiled=True)]
    ppermute x0 -> x15, starting transfers between devices: none -> 3.79 us  [body(): lax.ppermute(ring[-1], 'ep', [(dev, (dev + 1) % 16) for dev in range(16)])]
    all_to_all x1, starting transfers between devices: 4.19 us -> 7.01 us  [body(): lax.all_to_all(outgoing, 'ep', split_axis=0, concat_axis=0, tiled=True)]
  transfers between devices with their start and end apart: 5 -> 20, of which waited for: 4 -> 18; matrix products, arithmetic and copies ran while one was open for 8% -> 6% of each run, Pallas kernels for 0% -> 0%
where the time goes in v1:
time: 278 us; the launch traced here: 277 us
  waiting for transfers between devices  185 us (67%)
  blocking collectives  27.7 us (10%)
  matrix products  22.6 us (8%)
  between operations  14.4 us (5%)
  starting transfers between devices  11 us (4%)
  local copies, waits for them, and re-layouts  10.6 us (4%)
  other arithmetic  4.9 us (2%)
    ppermute x15, waiting for transfers between devices, body(): lax.ppermute(ring[-1], 'ep', [(dev, (dev + 1) % 16) for dev in range(16)])  96.7 us
    reduce_scatter x1, waiting for transfers between devices, body(): combined = lax.psum_scatter(value, 'ep', scatter_dimension=0, tiled=True)  63 us
    all_to_all x1, blocking collectives, body(): lax.all_to_all(served.astype(jnp.bfloat16), 'ep', split_axis=0, concat_ax...  18.1 us
    reduce_scatter x1, waiting for transfers between devices, body(): lax.psum_scatter(mix_part.astype(jnp.bfloat16), 'tp', scatter_dimension=1...  10.3 us
    reduce_scatter x1, waiting for transfers between devices, expert_apply(): lax.psum_scatter(partial_value.astype(jnp.bfloat16), 'tp', scatter_dimens...  8.79 us
    unnamed x106, local copies, waits for them, and re-layouts  7.5 us
    all_to_all x1, starting transfers between devices, body(): lax.all_to_all(outgoing, 'ep', split_axis=0, concat_axis=0, tiled=True)  7.01 us
    psum x1, waiting for transfers between devices, body(): lax.psum(up_pre.astype(jnp.bfloat16), 'tp').astype(jnp.float32)  6.51 us
  transfers between devices with their start and end apart: 20, of which 18 were waited for; matrix products, arithmetic and copies ran while one was open for 6% of the time, Pallas kernels for 0%

profile of v1, /device:TPU:0, one launch (start us, length us, event | category | flops | bytes accessed | tf_op | source)
XLA Modules:
  0.0 276.5 jit_solution(7475546766716763805)
XLA Ops:
  21.3 10.3 %reduce-scatter.4.cloned.1.call-done = bf16[16,1024]{1,0:T(8,128)(2,1)} async-done(((bf16[16,2048]{1,0:T(8,128)(2,1)}), bf16[16,1024]{1,0:T(8,128)(2,1)}) %reduce-scatter.4.cloned.1.call-update) | async-done | bytes 32784 | tf_op jit(solution)/shard_map/reduce_scatter | solution.py:97
  32.5 2.5 psum.28
  37.5 5.8 %collective-permute-done = bf16[16,1024]{1,0:T(8,128)(2,1)S(1)} collective-permute-done((bf16[16,1024]{1,0:T(8,128)(2,1)S(1)}, bf16[16,1024]{1,0:T(8,128)(2,1)S(1)}, u32[]{:S(2)}, u32[]{:S(2)}) %collective-permute-start) | collective-permute-done | bytes 32800 | tf_op jit(solution)/shard_map/ppermute | solution.py:107
  44.0 6.8 %collective-permute-done.1 = bf16[16,1024]{1,0:T(8,128)(2,1)S(1)} collective-permute-done((bf16[16,1024]{1,0:T(8,128)(2,1)S(1)}, bf16[16,1024]{1,0:T(8,128)(2,1)S(1)}, u32[]{:S(2)}, u32[]{:S(2)}) %collective-permute-start.1) | collective-permute-done | bytes 32800 | tf_op jit(solution)/shard_map/ppermute | solution.py:107
  50.9 7.4 %collective-permute-done.2 = bf16[16,1024]{1,0:T(8,128)(2,1)S(1)} collective-permute-done((bf16[16,1024]{1,0:T(8,128)(2,1)S(1)}, bf16[16,1024]{1,0:T(8,128)(2,1)S(1)}, u32[]{:S(2)}, u32[]{:S(2)}) %collective-permute-start.2) | collective-permute-done | bytes 32800 | tf_op jit(solution)/shard_map/ppermute | solution.py:107
  59.3 7.0 %all-to-all-start = ((bf16[16,5,1024]{2,1,0:T(8,128)(2,1)}), bf16[16,5,1024]{2,1,0:T(8,128)(2,1)S(1)}, u32[]{:S(2)}, u32[]{:S(2)}) async-start(bf16[16,5,1024]{2,1,0:T(8,128)(2,1)} %bitcast.9), calls=%async_computation.1 | async-start | bytes 524288 | tf_op jit(solution)/shard_map/all_to_all | solution.py:130
  68.3 7.7 %collective-permute-done.4 = bf16[16,1024]{1,0:T(8,128)(2,1)S(1)} collective-permute-done((bf16[16,1024]{1,0:T(8,128)(2,1)S(1)}, bf16[16,1024]{1,0:T(8,128)(2,1)S(1)}, u32[]{:S(2)}, u32[]{:S(2)}) %collective-permute-start.4) | collective-permute-done | bytes 32800 | tf_op jit(solution)/shard_map/ppermute | solution.py:107
  76.0 7.5 %collective-permute-done.5 = bf16[16,1024]{1,0:T(8,128)(2,1)S(1)} collective-permute-done((bf16[16,1024]{1,0:T(8,128)(2,1)S(1)}, bf16[16,1024]{1,0:T(8,128)(2,1)S(1)}, u32[]{:S(2)}, u32[]{:S(2)}) %collective-permute-start.5) | collective-permute-done | bytes 32800 | tf_op jit(solution)/shard_map/ppermute | solution.py:107
  83.5 7.5 %collective-permute-done.6 = bf16[16,1024]{1,0:T(8,128)(2,1)S(1)} collective-permute-done((bf16[16,1024]{1,0:T(8,128)(2,1)S(1)}, bf16[16,1024]{1,0:T(8,128)(2,1)S(1)}, u32[]{:S(2)}, u32[]{:S(2)}) %collective-permute-start.6) | collective-permute-done | bytes 32800 | tf_op jit(solution)/shard_map/ppermute | solution.py:107
  91.1 7.5 %collective-permute-done.7 = bf16[16,1024]{1,0:T(8,128)(2,1)S(1)} collective-permute-done((bf16[16,1024]{1,0:T(8,128)(2,1)S(1)}, bf16[16,1024]{1,0:T(8,128)(2,1)S(1)}, u32[]{:S(2)}, u32[]{:S(2)}) %collective-permute-start.7) | collective-permute-done | bytes 32800 | tf_op jit(solution)/shard_map/ppermute | solution.py:107
  98.6 7.5 %collective-permute-done.8 = bf16[16,1024]{1,0:T(8,128)(2,1)S(1)} collective-permute-done((bf16[16,1024]{1,0:T(8,128)(2,1)S(1)}, bf16[16,1024]{1,0:T(8,128)(2,1)S(1)}, u32[]{:S(2)}, u32[]{:S(2)}) %collective-permute-start.8) | collective-permute-done | bytes 32800 | tf_op jit(solution)/shard_map/ppermute | solution.py:107
  106.1 7.5 %collective-permute-done.9 = bf16[16,1024]{1,0:T(8,128)(2,1)S(1)} collective-permute-done((bf16[16,1024]{1,0:T(8,128)(2,1)S(1)}, bf16[16,1024]{1,0:T(8,128)(2,1)S(1)}, u32[]{:S(2)}, u32[]{:S(2)}) %collective-permute-start.9) | collective-permute-done | bytes 32800 | tf_op jit(solution)/shard_map/ppermute | solution.py:107
  113.6 7.5 %collective-permute-done.10 = bf16[16,1024]{1,0:T(8,128)(2,1)S(1)} collective-permute-done((bf16[16,1024]{1,0:T(8,128)(2,1)S(1)}, bf16[16,1024]{1,0:T(8,128)(2,1)S(1)}, u32[]{:S(2)}, u32[]{:S(2)}) %collective-permute-start.10) | collective-permute-done | bytes 32800 | tf_op jit(solution)/shard_map/ppermute | solution.py:107
  121.1 7.6 %collective-permute-done.11 = bf16[16,1024]{1,0:T(8,128)(2,1)} collective-permute-done((bf16[16,1024]{1,0:T(8,128)(2,1)S(1)}, bf16[16,1024]{1,0:T(8,128)(2,1)}, u32[]{:S(2)}, u32[]{:S(2)}) %collective-permute-start.11) | collective-permute-done | bytes 32800 | tf_op jit(solution)/shard_map/ppermute | solution.py:107
  129.3 7.2 %collective-permute-done.12 = bf16[16,1024]{1,0:T(8,128)(2,1)} collective-permute-done((bf16[16,1024]{1,0:T(8,128)(2,1)}, bf16[16,1024]{1,0:T(8,128)(2,1)}, u32[]{:S(2)}, u32[]{:S(2)}) %collective-permute-start.12) | collective-permute-done | bytes 32800 | tf_op jit(solution)/shard_map/ppermute | solution.py:107
  140.1 4.2 %collective-permute-done.13 = bf16[16,1024]{1,0:T(8,128)(2,1)} collective-permute-done((bf16[16,1024]{1,0:T(8,128)(2,1)}, bf16[16,1024]{1,0:T(8,128)(2,1)}, u32[]{:S(2)}, u32[]{:S(2)}) %collective-permute-start.13) | collective-permute-done | bytes 32800 | tf_op jit(solution)/shard_map/ppermute | solution.py:107
  144.6 2.8 %fusion.4 = f32[80,704]{1,0:T(8,128)S(1)} fusion(bf16[80,2048]{1,0:T(8,128)(2,1)S(1)} %reshape.74, bf16[1,2048,704]{1,2,0:T(8,128)(2,1)} %param.29), kind=kOutput, calls=%fused_computation.4 | convolution fusion | flops 230686720 | bytes 3436544 | tf_op jit(solution)/shard_map/dot_general | solution.py:26
  147.4 4.8 %collective-permute-done.14 = bf16[16,1024]{1,0:T(8,128)(2,1)S(1)} collective-permute-done((bf16[16,1024]{1,0:T(8,128)(2,1)}, bf16[16,1024]{1,0:T(8,128)(2,1)S(1)}, u32[]{:S(2)}, u32[]{:S(2)}) %collective-permute-start.14) | collective-permute-done | bytes 32800 | tf_op jit(solution)/shard_map/ppermute | solution.py:107
  160.0 4.4 %fusion.6 = bf16[80,2048]{1,0:T(8,128)(2,1)} fusion(bf16[1,704,2048]{2,1,0:T(8,128)(2,1)S(1)} %copy-done, bf16[80,2048]{1,0:T(8,128)(2,1)S(1)} %reshape.74, bf16[1,2048,704]{1,2,0:T(8,128)(2,1)} %param.30, f32[80,704]{1,0:T(8,128)S(1)} %fusion.4), kind=kOutput, calls=%fused_computation.6 | convolution fusion | flops 461875200 | bytes 6647808 | tf_op jit(solution)/shard_map/dot_general | solution.py:29
  165.8 2.4 psum.29
  168.3 6.5 %all-reduce.3.cloned.1.call-done = (bf16[256,176]{0,1:T(8,128)(2,1)}, bf16[256,176]{0,1:T(8,128)(2,1)}) async-done(((bf16[256,176]{0,1:T(8,128)(2,1)}, bf16[256,176]{0,1:T(8,128)(2,1)}), (bf16[256,176]{0,1:T(8,128)(2,1)}, bf16[256,176]{0,1:T(8,128)(2,1)})) %all-reduce.3.cloned.1.call-update) | async-done | bytes 180240 | tf_op jit(solution)/shard_map/psum | solution.py:116
  177.3 8.8 %reduce-scatter.6.cloned.1.call-done = bf16[80,1024]{1,0:T(8,128)(2,1)} async-done(((bf16[80,2048]{1,0:T(8,128)(2,1)}), bf16[80,1024]{1,0:T(8,128)(2,1)}) %reduce-scatter.6.cloned.1.call-update) | async-done | bytes 163856 | tf_op jit(solution)/shard_map/reduce_scatter | solution.py:36
  187.0 18.1 %all_to_all.10 = bf16[16,5,1024]{2,1,0:T(8,128)(2,1)S(1)} all-to-all(bf16[16,5,1024]{2,1,0:T(8,128)(2,1)S(1)} %convert_element_type.118), channel_id=1, replica_groups=mesh['ep'=16,'tp'=2] {'ep'}, dimensions={0} | all-to-all | bytes 327680 | tf_op jit(solution)/shard_map/all_to_all | solution.py:132
  205.2 63.0 %reduce-scatter.8.cloned.1.call-done = f32[16,1024]{1,0:T(8,128)} async-done(((f32[256,1024]{1,0:T(8,128)}), f32[16,1024]{1,0:T(8,128)}) %reduce-scatter.8.cloned.1.call-update) | async-done | bytes 65552 | tf_op jit(solution)/shard_map/reduce_scatter | solution.py:140
  (173 shorter events, 39.6 us)
Async XLA Ops:
  7.2 152.9 %copy-start = (bf16[1,704,2048]{2,1,0:T(8,128)(2,1)S(1)}, bf16[1,704,2048]{2,1,0:T(8,128)(2,1)}, u32[]{:S(2)}) copy-start(bf16[1,704,2048]{2,1,0:T(8,128)(2,1)} %param.31) | copy-start | bytes 8650756
  7.2 24.4 %reduce-scatter.4.cloned.1.call-start = ((), (), s32[]{:S(2)}) async-start(), calls=%async_computation.5 | async-start | bytes 98304 | tf_op jit(solution)/shard_map/reduce_scatter | solution.py:97
  17.7 111.0 %copy-start.34 = (bf16[1024]{0:T(1024)(128)(2,1)S(1)}, bf16[1024]{0:T(1024)(128)(2,1)}, u32[]{:S(2)}) copy-start(bf16[1024]{0:T(1024)(128)(2,1)} %param.25) | copy-start | bytes 6148
  35.8 7.5 %collective-permute-start = (bf16[16,1024]{1,0:T(8,128)(2,1)S(1)}, bf16[16,1024]{1,0:T(8,128)(2,1)S(1)}, u32[]{:S(2)}, u32[]{:S(2)}) collective-permute-start(bf16[16,1024]{1,0:T(8,128)(2,1)S(1)} %fusion.49), channel_id=1, source_target_pairs={{0,2},{2,4},{4,6},{6,8},{8,10},{10,12},{12,14},{14,16},{16,18},{18... | collective-permute-start | bytes 98312 | tf_op jit(solution)/shard_map/ppermute | solution.py:107
  43.3 7.5 %collective-permute-start.1 = (bf16[16,1024]{1,0:T(8,128)(2,1)S(1)}, bf16[16,1024]{1,0:T(8,128)(2,1)S(1)}, u32[]{:S(2)}, u32[]{:S(2)}) collective-permute-start(bf16[16,1024]{1,0:T(8,128)(2,1)S(1)} %collective-permute-done), channel_id=1, source_target_pairs={{0,2},{2,4},{4,6},{6,8},{8,10},{10,12},{12,14},{14,16},{16,18},{18... | collective-permute-start | bytes 98312 | tf_op jit(solution)/shard_map/ppermute | solution.py:107
  50.8 7.5 %collective-permute-start.2 = (bf16[16,1024]{1,0:T(8,128)(2,1)S(1)}, bf16[16,1024]{1,0:T(8,128)(2,1)S(1)}, u32[]{:S(2)}, u32[]{:S(2)}) collective-permute-start(bf16[16,1024]{1,0:T(8,128)(2,1)S(1)} %collective-permute-done.1), channel_id=1, source_target_pairs={{0,2},{2,4},{4,6},{6,8},{8,10},{10,12},{12,14},{14,16},{16,18},{18... | collective-permute-start | bytes 98312 | tf_op jit(solution)/shard_map/ppermute | solution.py:107
  58.3 8.0 %collective-permute-start.3 = (bf16[16,1024]{1,0:T(8,128)(2,1)S(1)}, bf16[16,1024]{1,0:T(8,128)(2,1)S(1)}, u32[]{:S(2)}, u32[]{:S(2)}) collective-permute-start(bf16[16,1024]{1,0:T(8,128)(2,1)S(1)} %collective-permute-done.2), channel_id=1, source_target_pairs={{0,2},{2,4},{4,6},{6,8},{8,10},{10,12},{12,14},{14,16},{16,18},{18... | collective-permute-start | bytes 98312 | tf_op jit(solution)/shard_map/ppermute | solution.py:107
  59.3 77.3 %all-to-all-start = ((bf16[16,5,1024]{2,1,0:T(8,128)(2,1)}), bf16[16,5,1024]{2,1,0:T(8,128)(2,1)S(1)}, u32[]{:S(2)}, u32[]{:S(2)}) async-start(bf16[16,5,1024]{2,1,0:T(8,128)(2,1)} %bitcast.9), calls=%async_computation.1 | async-start | bytes 524288 | tf_op jit(solution)/shard_map/all_to_all | solution.py:130
  66.3 108.5 %all-reduce.3.cloned.1.call-start = ((), (), s32[]{:S(2)}) async-start(), calls=%async_computation.8 | async-start | bytes 360448 | tf_op jit(solution)/shard_map/psum | solution.py:116
  66.4 9.7 %collective-permute-start.4 = (bf16[16,1024]{1,0:T(8,128)(2,1)S(1)}, bf16[16,1024]{1,0:T(8,128)(2,1)S(1)}, u32[]{:S(2)}, u32[]{:S(2)}) collective-permute-start(bf16[16,1024]{1,0:T(8,128)(2,1)S(1)} %collective-permute-done.3), channel_id=1, source_target_pairs={{0,2},{2,4},{4,6},{6,8},{8,10},{10,12},{12,14},{14,16},{16,18},{18... | collective-permute-start | bytes 98312 | tf_op jit(solution)/shard_map/ppermute | solution.py:107
  76.0 7.5 %collective-permute-start.5 = (bf16[16,1024]{1,0:T(8,128)(2,1)S(1)}, bf16[16,1024]{1,0:T(8,128)(2,1)S(1)}, u32[]{:S(2)}, u32[]{:S(2)}) collective-permute-start(bf16[16,1024]{1,0:T(8,128)(2,1)S(1)} %collective-permute-done.4), channel_id=1, source_target_pairs={{0,2},{2,4},{4,6},{6,8},{8,10},{10,12},{12,14},{14,16},{16,18},{18... | collective-permute-start | bytes 98312 | tf_op jit(solution)/shard_map/ppermute | solution.py:107
  83.5 7.5 %collective-permute-start.6 = (bf16[16,1024]{1,0:T(8,128)(2,1)S(1)}, bf16[16,1024]{1,0:T(8,128)(2,1)S(1)}, u32[]{:S(2)}, u32[]{:S(2)}) collective-permute-start(bf16[16,1024]{1,0:T(8,128)(2,1)S(1)} %collective-permute-done.5), channel_id=1, source_target_pairs={{0,2},{2,4},{4,6},{6,8},{8,10},{10,12},{12,14},{14,16},{16,18},{18... | collective-permute-start | bytes 98312 | tf_op jit(solution)/shard_map/ppermute | solution.py:107
  91.1 7.5 %collective-permute-start.7 = (bf16[16,1024]{1,0:T(8,128)(2,1)S(1)}, bf16[16,1024]{1,0:T(8,128)(2,1)S(1)}, u32[]{:S(2)}, u32[]{:S(2)}) collective-permute-start(bf16[16,1024]{1,0:T(8,128)(2,1)S(1)} %collective-permute-done.6), channel_id=1, source_target_pairs={{0,2},{2,4},{4,6},{6,8},{8,10},{10,12},{12,14},{14,16},{16,18},{18... | collective-permute-start | bytes 98312 | tf_op jit(solution)/shard_map/ppermute | solution.py:107
  98.6 7.5 %collective-permute-start.8 = (bf16[16,1024]{1,0:T(8,128)(2,1)S(1)}, bf16[16,1024]{1,0:T(8,128)(2,1)S(1)}, u32[]{:S(2)}, u32[]{:S(2)}) collective-permute-start(bf16[16,1024]{1,0:T(8,128)(2,1)S(1)} %collective-permute-done.7), channel_id=1, source_target_pairs={{0,2},{2,4},{4,6},{6,8},{8,10},{10,12},{12,14},{14,16},{16,18},{18... | collective-permute-start | bytes 98312 | tf_op jit(solution)/shard_map/ppermute | solution.py:107
  106.1 7.5 %collective-permute-start.9 = (bf16[16,1024]{1,0:T(8,128)(2,1)S(1)}, bf16[16,1024]{1,0:T(8,128)(2,1)S(1)}, u32[]{:S(2)}, u32[]{:S(2)}) collective-permute-start(bf16[16,1024]{1,0:T(8,128)(2,1)S(1)} %collective-permute-done.8), channel_id=1, source_target_pairs={{0,2},{2,4},{4,6},{6,8},{8,10},{10,12},{12,14},{14,16},{16,18},{18... | collective-permute-start | bytes 98312 | tf_op jit(solution)/shard_map/ppermute | solution.py:107
  113.6 7.5 %collective-permute-start.10 = (bf16[16,1024]{1,0:T(8,128)(2,1)S(1)}, bf16[16,1024]{1,0:T(8,128)(2,1)S(1)}, u32[]{:S(2)}, u32[]{:S(2)}) collective-permute-start(bf16[16,1024]{1,0:T(8,128)(2,1)S(1)} %collective-permute-done.9), channel_id=1, source_target_pairs={{0,2},{2,4},{4,6},{6,8},{8,10},{10,12},{12,14},{14,16},{16,18},{18... | collective-permute-start | bytes 98312 | tf_op jit(solution)/shard_map/ppermute | solution.py:107
  121.1 7.6 %collective-permute-start.11 = (bf16[16,1024]{1,0:T(8,128)(2,1)S(1)}, bf16[16,1024]{1,0:T(8,128)(2,1)}, u32[]{:S(2)}, u32[]{:S(2)}) collective-permute-start(bf16[16,1024]{1,0:T(8,128)(2,1)S(1)} %collective-permute-done.10), channel_id=1, source_target_pairs={{0,2},{2,4},{4,6},{6,8},{8,10},{10,12},{12,14},{14,16},{16,18},{18... | collective-permute-start | bytes 98312 | tf_op jit(solution)/shard_map/ppermute | solution.py:107
  128.7 7.8 %collective-permute-start.12 = (bf16[16,1024]{1,0:T(8,128)(2,1)}, bf16[16,1024]{1,0:T(8,128)(2,1)}, u32[]{:S(2)}, u32[]{:S(2)}) collective-permute-start(bf16[16,1024]{1,0:T(8,128)(2,1)} %collective-permute-done.11), channel_id=1, source_target_pairs={{0,2},{2,4},{4,6},{6,8},{8,10},{10,12},{12,14},{14,16},{16,18},{18... | collective-permute-start | bytes 98312 | tf_op jit(solution)/shard_map/ppermute | solution.py:107
  136.6 7.8 %collective-permute-start.13 = (bf16[16,1024]{1,0:T(8,128)(2,1)}, bf16[16,1024]{1,0:T(8,128)(2,1)}, u32[]{:S(2)}, u32[]{:S(2)}) collective-permute-start(bf16[16,1024]{1,0:T(8,128)(2,1)} %collective-permute-done.12), channel_id=1, source_target_pairs={{0,2},{2,4},{4,6},{6,8},{8,10},{10,12},{12,14},{14,16},{16,18},{18... | collective-permute-start | bytes 98312 | tf_op jit(solution)/shard_map/ppermute | solution.py:107
  144.4 7.8 %collective-permute-start.14 = (bf16[16,1024]{1,0:T(8,128)(2,1)}, bf16[16,1024]{1,0:T(8,128)(2,1)S(1)}, u32[]{:S(2)}, u32[]{:S(2)}) collective-permute-start(bf16[16,1024]{1,0:T(8,128)(2,1)} %collective-permute-done.13), channel_id=1, source_target_pairs={{0,2},{2,4},{4,6},{6,8},{8,10},{10,12},{12,14},{14,16},{16,18},{18... | collective-permute-start | bytes 98312 | tf_op jit(solution)/shard_map/ppermute | solution.py:107
  160.0 26.1 %reduce-scatter.6.cloned.1.call-start = ((), (), s32[]{:S(2)}) async-start(), calls=%async_computation.6 | async-start | bytes 491520 | tf_op jit(solution)/shard_map/reduce_scatter | solution.py:36
  164.4 103.8 %copy-start.30 = (f32[8,16]{1,0:T(8,128)S(1)}, f32[8,16]{1,0:T(8,128)}, u32[]{:S(2)}) copy-start(f32[8,16]{1,0:T(8,128)} %copy-done.29) | copy-start | bytes 1540
  164.4 103.8 %copy-start.31 = (f32[16,8]{0,1:T(8,128)S(1)}, f32[16,8]{0,1:T(8,128)}, u32[]{:S(2)}) copy-start(f32[16,8]{0,1:T(8,128)} %get-tuple-element.2) | copy-start | bytes 1540
  164.5 103.8 %reduce-scatter.8.cloned.1.call-start = ((), (), s32[]{:S(2)}) async-start(), calls=%async_computation.7 | async-start | bytes 1114112 | tf_op jit(solution)/shard_map/reduce_scatter | solution.py:140
  (33 other events, 959.5 us)
Sparse Core Ops, SparseCore 0:
  21.4 10.1 reduce-scatter.3
  160.1 14.6 all-reduce.2
  177.0 8.9 reduce-scatter.5
  188.2 80.0 reduce-scatter.7
